TPU v7x, 512 devices: a whole 4x4x16 slice. The times are simulated.
512 devices in a mesh: fs: 32 (over z, core), tp: 16 (over y, x).
Axes of the slice: x: 4, y: 4, z: 16, core: 2. Of those that a mesh axis runs over, the one named last changes fastest.
Arguments:
- late_input: bfloat16 [4096, 2048], P('fs'), may hold values from -6 to 6
- early_input: bfloat16 [4096, 2048], P('fs'), may hold values from -6 to 6
- early_mid: bfloat16 [4096, 2048], P('fs'), may hold values from -6 to 6
- cotangent: bfloat16 [4096, 2048], P('fs'), may hold values from -6 to 6
- gain_first: float32 [2048], replicated, may hold values from 0.1 to 1.9
- gain_second: float32 [2048], replicated, may hold values from 0.1 to 1.9
- gate_first: bfloat16 [2048, 2816], P('fs', 'tp'), may hold values from -0.125 to 0.125
- up_first: bfloat16 [2048, 2816], P('fs', 'tp'), may hold values from -0.125 to 0.125
- down_first: bfloat16 [2816, 2048], P('tp', 'fs'), may hold values from -0.109375 to 0.109375
- gate_second: bfloat16 [2048, 2816], P('fs', 'tp'), may hold values from -0.125 to 0.125
- up_second: bfloat16 [2048, 2816], P('fs', 'tp'), may hold values from -0.125 to 0.125
- down_second: bfloat16 [2816, 2048], P('tp', 'fs'), may hold values from -0.109375 to 0.109375
- sum_gate_first: float32 [2048, 2816], P('fs', 'tp'), may hold values from -256 to 256
- sum_up_first: float32 [2048, 2816], P('fs', 'tp'), may hold values from -256 to 256
- sum_down_first: float32 [2816, 2048], P('tp', 'fs'), may hold values from -256 to 256
- sum_gate_second: float32 [2048, 2816], P('fs', 'tp'), may hold values from -256 to 256
- sum_up_second: float32 [2048, 2816], P('fs', 'tp'), may hold values from -256 to 256
- sum_down_second: float32 [2816, 2048], P('tp', 'fs'), may hold values from -256 to 256
Outputs:
- late_mid: bfloat16 [4096, 2048], P('fs')
- late_out: bfloat16 [4096, 2048], P('fs')
- input_grad: bfloat16 [4096, 2048], P('fs')
- new_gate_first: float32 [2048, 2816], P('fs', 'tp')
- new_up_first: float32 [2048, 2816], P('fs', 'tp')
- new_down_first: float32 [2816, 2048], P('tp', 'fs')
- new_gate_second: float32 [2048, 2816], P('fs', 'tp')
- new_up_second: float32 [2048, 2816], P('fs', 'tp')
- new_down_second: float32 [2816, 2048], P('tp', 'fs')
All inputs are finite; a program needn't handle non-finite values.
Results may differ from a plain program's by a relative error of at most 0.015.
Values may be sent and summed in bfloat16 or wider, within the bound.
No kernel may reach another device: no remote copies, remote signals or barrier semaphores. Data moves between devices by JAX's collectives and lax.ppermute only.
A program may use at most 128 MiB of HBM per device.

v0:
```python
import jax
import jax.numpy as jnp
from jax import lax
from jax.sharding import PartitionSpec as P

norm_eps = 1e-06


def sent_together(arrays, axis, dim, along):
    both = jnp.concatenate(arrays, axis=along)
    whole, at, outs = (lax.all_gather(both, axis, axis=dim, tiled=True), 0, [])
    for a in arrays:
        outs.append(lax.slice_in_dim(whole, at, at + a.shape[along], axis=along))
        at += a.shape[along]
    return tuple(outs)


def gather_turned(arrays, axis, dims):
    turned = [jnp.moveaxis(a, dim, 0) for a, dim in zip(arrays, dims)]
    widths = [t[0].size for t in turned]
    both = jnp.concatenate([t.reshape(-1, w) for t, w in zip(turned, widths)], axis=1)
    whole = lax.all_gather(both, axis, axis=0, tiled=True)
    blocks = jnp.split(whole, [sum(widths[:k]) for k in range(1, len(widths))], axis=1)
    return tuple(
        (
            jnp.moveaxis(b.reshape(-1, *t.shape[1:]), 0, dim)
            for b, t, dim in zip(blocks, turned, dims)
        )
    )


def normalize(values, gain_vector):
    widened = values.astype(jnp.float32)
    factor = lax.rsqrt(jnp.mean(widened * widened, axis=-1, keepdims=True) + norm_eps)
    normed = (widened * factor * gain_vector).astype(jnp.bfloat16)
    return (widened, factor, normed)


def block_forward(values, params):
    gain_vector, w_gate, w_up, w_down = params
    widened, factor, normed = normalize(values, gain_vector)
    gate_pre = jnp.dot(normed, w_gate, preferred_element_type=jnp.float32)
    up_pre = jnp.dot(normed, w_up, preferred_element_type=jnp.float32)
    hidden = (jax.nn.silu(gate_pre) * up_pre).astype(jnp.bfloat16)
    branch = lax.psum(
        jnp.dot(hidden, w_down, preferred_element_type=jnp.float32).astype(jnp.bfloat16), "tp"
    ).astype(jnp.float32)
    return (widened + 0.5 * branch).astype(jnp.bfloat16)


def block_backward(values, cotangent, params):
    gain_vector, w_gate, w_up, w_down = params
    widened, factor, normed = normalize(values, gain_vector)
    gate_pre = jnp.dot(normed, w_gate, preferred_element_type=jnp.float32)
    up_pre = jnp.dot(normed, w_up, preferred_element_type=jnp.float32)
    sigmoid_gate = jax.nn.sigmoid(gate_pre)
    activated = gate_pre * sigmoid_gate
    hidden = (activated * up_pre).astype(jnp.bfloat16)
    hidden_grad = 0.5 * jnp.einsum(
        "td,fd->tf", cotangent, w_down, preferred_element_type=jnp.float32
    )
    gate_grad = (
        hidden_grad * up_pre * sigmoid_gate * (1.0 + gate_pre * (1.0 - sigmoid_gate))
    ).astype(jnp.bfloat16)
    up_grad = (hidden_grad * activated).astype(jnp.bfloat16)
    partial_value = jnp.einsum("tf,df->td", gate_grad, w_gate, preferred_element_type=jnp.float32)
    partial_value = partial_value + jnp.einsum(
        "tf,df->td", up_grad, w_up, preferred_element_type=jnp.float32
    )
    normed_grad = lax.psum(partial_value.astype(jnp.bfloat16), "tp").astype(jnp.float32)
    scaled = normed_grad * gain_vector
    unit_rows = widened * factor
    rows_grad = cotangent.astype(jnp.float32) + factor * (
        scaled - unit_rows * jnp.mean(scaled * unit_rows, axis=-1, keepdims=True)
    )
    return (rows_grad, (normed, cotangent, gate_grad, up_grad, hidden))


def fold_pair(pieces, columns_in):
    return (
        jnp.einsum("td,tf->df", columns_in, pieces[0], preferred_element_type=jnp.float32),
        jnp.einsum("td,tf->df", columns_in, pieces[1], preferred_element_type=jnp.float32),
    )


def fold_block(pieces, columns_in, columns_out):
    paired = fold_pair(pieces[0:2], columns_in)
    return paired + (
        jnp.einsum("tf,td->fd", pieces[2], columns_out, preferred_element_type=jnp.float32),
    )


def per_device(
    late_input,
    early_input,
    early_mid,
    cotangent,
    gain_first,
    gain_second,
    gate_first,
    up_first,
    down_first,
    gate_second,
    up_second,
    down_second,
    sum_gate_first,
    sum_up_first,
    sum_down_first,
    sum_gate_second,
    sum_up_second,
    sum_down_second,
):
    rows_in = sent_together((gate_first, up_first, gate_second, up_second), "fs", 0, 1)
    cols_out = gather_turned((down_first, down_second), "fs", (1, 1))
    first_params = (gain_first, rows_in[0], rows_in[1], cols_out[0])
    second_params = (gain_second, rows_in[2], rows_in[3], cols_out[1])
    late_mid = block_forward(late_input, first_params)
    late_out = block_forward(late_mid, second_params)
    mid_grad, saved_second = block_backward(early_mid, cotangent, second_params)
    mid_grad = mid_grad.astype(jnp.bfloat16)
    rows_grad, saved_first = block_backward(early_input, mid_grad, first_params)
    pieces = sent_together(
        (
            saved_second[2],
            saved_second[3],
            saved_second[4],
            saved_first[2],
            saved_first[3],
            saved_first[4],
        ),
        "fs",
        0,
        1,
    )
    upper = fold_block(
        pieces[0:3],
        lax.all_to_all(saved_second[0], "fs", split_axis=1, concat_axis=0, tiled=True),
        lax.all_to_all(saved_second[1], "fs", split_axis=1, concat_axis=0, tiled=True),
    )
    lower = fold_block(
        pieces[3:6],
        lax.all_to_all(saved_first[0], "fs", split_axis=1, concat_axis=0, tiled=True),
        lax.all_to_all(saved_first[1], "fs", split_axis=1, concat_axis=0, tiled=True),
    )
    result = upper + lower
    grads_second = (result[0], result[1], 0.5 * result[2])
    grads_first = (result[3], result[4], 0.5 * result[5])
    return (
        late_mid,
        late_out,
        rows_grad.astype(jnp.bfloat16),
        sum_gate_first + grads_first[0],
        sum_up_first + grads_first[1],
        sum_down_first + grads_first[2],
        sum_gate_second + grads_second[0],
        sum_up_second + grads_second[1],
        sum_down_second + grads_second[2],
    )


def solution(mesh):
    in_specs = (
        P("fs", None),
        P("fs", None),
        P("fs", None),
        P("fs", None),
        P(),
        P(),
        P("fs", "tp"),
        P("fs", "tp"),
        P("tp", "fs"),
        P("fs", "tp"),
        P("fs", "tp"),
        P("tp", "fs"),
        P("fs", "tp"),
        P("fs", "tp"),
        P("tp", "fs"),
        P("fs", "tp"),
        P("fs", "tp"),
        P("tp", "fs"),
    )
    out_specs = (
        P("fs", None),
        P("fs", None),
        P("fs", None),
        P("fs", "tp"),
        P("fs", "tp"),
        P("tp", "fs"),
        P("fs", "tp"),
        P("fs", "tp"),
        P("tp", "fs"),
    )
    return jax.shard_map(
        per_device, mesh=mesh, in_specs=in_specs, out_specs=out_specs, check_vma=False
    )
```

profile of v0, /device:TPU:1, one launch (start us, length us, event | category | flops | bytes accessed | tf_op | source)
XLA Modules:
  0.0 560.9 jit_solution(5887314163387625684)
XLA Ops:
  7.2 1.5 pad_maximum_fusion.1
  8.8 1.6 pad_maximum_fusion
  10.4 1.2 fusion.61
  11.6 1.2 fusion.53
  12.9 1.2 fusion.60
  14.1 2.0 fusion.47
  16.1 71.3 %all-gather.6.cloned.1.call-done = bf16[2048,352]{1,0:T(8,128)(2,1)} async-done(((bf16[64,352]{1,0:T(8,128)(2,1)}), bf16[2048,352]{1,0:T(8,128)(2,1)}) %all-gather.6.cloned.1.call-update) | async-done | bytes 1441808 | tf_op jit(solution)/shard_map/all_gather | solution.py:22
  87.5 2.1 fusion.20
  89.6 70.4 %all-gather.4.cloned.1.call-done = bf16[2048,704]{1,0:T(8,128)(2,1)} async-done(((bf16[64,704]{1,0:T(8,128)(2,1)}), bf16[2048,704]{1,0:T(8,128)(2,1)}) %all-gather.4.cloned.1.call-update) | async-done | bytes 2883600 | tf_op jit(solution)/shard_map/all_gather | solution.py:11
  160.0 2.6 fusion.74
  162.6 3.2 constant_dynamic-update-slice_fusion.3
  166.5 1.6 fusion.93
  168.1 3.9 convolution_convert_fusion.1
  172.0 0.7 fusion.78
  172.6 1.5 fusion
  174.4 1.2 fusion.54
  175.6 0.8 fusion.125
  176.5 1.0 fusion.85
  177.5 110.1 %all-reduce.7.cloned.1.call-done = (bf16[128,2048]{1,0:T(8,128)(2,1)}, bf16[128,2048]{1,0:T(8,128)(2,1)}) async-done(((bf16[128,2048]{1,0:T(8,128)(2,1)}, bf16[128,2048]{1,0:T(8,128)(2,1)}), (bf16[128,2048]{1,0:T(8,128)(2,1)}, bf16[128,2048]{1,0:T(8,128)(2,1)})) %all-reduce.7.cloned.1.call-update) | async-done | bytes 1048592 | tf_op jit(solution)/shard_map/psum | solution.py:45
  287.6 1.7 fusion.65
  289.3 1.7 fusion.48
  291.0 1.8 fusion.52
  292.8 0.8 copy-done.2
  294.1 1.1 constant_dynamic-update-slice_fusion.1
  295.9 1.7 fusion.82
  297.6 4.0 convolution_convert_fusion
  302.1 1.5 fusion.1
  304.3 2.1 copy.27
  306.4 14.7 %all-to-all-start = ((bf16[128,32,64]{0,2,1:T(8,128)(2,1)}), bf16[128,32,64]{0,2,1:T(8,128)(2,1)S(1)}, u32[]{:S(2)}, u32[]{:S(2)}) async-start(bf16[128,32,64]{0,2,1:T(8,128)(2,1)} %bitcast.3), calls=%async_computation | async-start | bytes 1048576 | tf_op jit(solution)/shard_map/all_to_all | solution.py:142
  321.1 1.0 copy.31
  322.2 32.5 %all-to-all-done = bf16[128,32,64]{0,2,1:T(8,128)(2,1)S(1)} async-done(((bf16[128,32,64]{0,2,1:T(8,128)(2,1)}), bf16[128,32,64]{0,2,1:T(8,128)(2,1)S(1)}, u32[]{:S(2)}, u32[]{:S(2)}) %all-to-all-start) | async-done | bytes 524320 | tf_op jit(solution)/shard_map/all_to_all | solution.py:142
  354.6 4.2 all-to-all-start.2
  358.8 1.0 copy.29
  359.8 32.5 %all-to-all-done.2 = bf16[128,32,64]{0,2,1:T(8,128)(2,1)S(1)} async-done(((bf16[128,32,64]{0,2,1:T(8,128)(2,1)}), bf16[128,32,64]{0,2,1:T(8,128)(2,1)S(1)}, u32[]{:S(2)}, u32[]{:S(2)}) %all-to-all-start.2) | async-done | bytes 524320 | tf_op jit(solution)/shard_map/all_to_all | solution.py:137
  392.3 5.0 all-to-all-start.1
  397.4 1.0 copy.33
  398.4 22.9 %all-reduce.5.cloned.1.call-done = (bf16[128,2048]{1,0:T(8,128)(2,1)}, bf16[128,2048]{1,0:T(8,128)(2,1)}) async-done(((bf16[128,2048]{1,0:T(8,128)(2,1)}, bf16[128,2048]{1,0:T(8,128)(2,1)}), (bf16[128,2048]{1,0:T(8,128)(2,1)}, bf16[128,2048]{1,0:T(8,128)(2,1)})) %all-reduce.5.cloned.1.call-update) | async-done | bytes 1048592 | tf_op jit(solution)/shard_map/psum | solution.py:45
  421.2 1.4 fusion.55
  422.6 8.3 %all-to-all-done.1 = bf16[128,32,64]{0,2,1:T(8,128)(2,1)} async-done(((bf16[128,32,64]{0,2,1:T(8,128)(2,1)}), bf16[128,32,64]{0,2,1:T(8,128)(2,1)}, u32[]{:S(2)}, u32[]{:S(2)}) %all-to-all-start.1) | async-done | bytes 524320 | tf_op jit(solution)/shard_map/all_to_all | solution.py:143
  430.9 6.1 %all-to-all-start.3 = ((bf16[128,32,64]{0,2,1:T(8,128)(2,1)}), bf16[128,32,64]{0,2,1:T(8,128)(2,1)S(1)}, u32[]{:S(2)}, u32[]{:S(2)}) async-start(bf16[128,32,64]{0,2,1:T(8,128)(2,1)} %bitcast.9), calls=%async_computation.3 | async-start | bytes 1048576 | tf_op jit(solution)/shard_map/all_to_all | solution.py:138
  437.1 2.7 fusion.59
  439.8 98.8 %all-gather.8.cloned.1.call-done = bf16[4096,1056]{0,1:T(8,128)(2,1)} async-done(((bf16[128,1056]{0,1:T(8,128)(2,1)}), bf16[4096,1056]{0,1:T(8,128)(2,1)}) %all-gather.8.cloned.1.call-update) | async-done | bytes 8650768 | tf_op jit(solution)/shard_map/all_gather | solution.py:11
  538.7 2.6 fusion.23
  541.2 2.6 fusion.26
  543.9 2.6 fusion.35
  546.4 2.6 fusion.38
  549.1 2.7 fusion.32
  551.8 2.6 fusion.44
  (59 shorter events, 3.6 us)
Async XLA Ops:
  7.2 80.3 %all-gather.6.cloned.1.call-start = ((), (), s32[]{:S(2)}) async-start(), calls=%async_computation.5 | async-start | bytes 1622016 | tf_op jit(solution)/shard_map/all_gather | solution.py:22
  8.7 151.3 %all-gather.4.cloned.1.call-start = ((), (), s32[]{:S(2)}) async-start(), calls=%async_computation.4 | async-start | bytes 3244032 | tf_op jit(solution)/shard_map/all_gather | solution.py:11
  10.4 277.2 %all-reduce.7.cloned.1.call-start = ((), (), s32[]{:S(2)}) async-start(), calls=%async_computation.8 | async-start | bytes 2097152 | tf_op jit(solution)/shard_map/psum | solution.py:45
  16.1 150.4 %copy-start.12 = (f32[2048]{0:T(1024)S(1)}, f32[2048]{0:T(1024)}, u32[]{:S(2)}) copy-start(f32[2048]{0:T(1024)} %param.22) | copy-start | bytes 24580
  160.0 6.5 %copy-start = (bf16[2048,704]{1,0:T(8,128)(2,1)S(1)}, bf16[2048,704]{1,0:T(8,128)(2,1)}, u32[]{:S(2)}) copy-start(bf16[2048,704]{1,0:T(8,128)(2,1)} %all-gather.4.cloned.1.call-done) | copy-start | bytes 8650756
  174.1 115.2 %copy-start.11 = (f32[2048]{0:T(1024)S(1)}, f32[2048]{0:T(1024)}, u32[]{:S(2)}) copy-start(f32[2048]{0:T(1024)} %param.23) | copy-start | bytes 24580
  174.1 247.1 %all-reduce.5.cloned.1.call-start = ((), (), s32[]{:S(2)}) async-start(), calls=%async_computation.7 | async-start | bytes 2097152 | tf_op jit(solution)/shard_map/psum | solution.py:45
  175.6 0.9 copy-start.5
  287.6 6.0 %copy-start.10 = (bf16[2048,352]{1,0:T(8,128)(2,1)S(1)}, bf16[2048,352]{1,0:T(8,128)(2,1)}, u32[]{:S(2)}) copy-start(bf16[2048,352]{1,0:T(8,128)(2,1)} %all-gather.6.cloned.1.call-done) | copy-start | bytes 4325380
  287.6 6.5 %copy-start.6 = (bf16[128,2048]{1,0:T(8,128)(2,1)S(1)}, bf16[128,2048]{1,0:T(8,128)(2,1)}, u32[]{:S(2)}) copy-start(bf16[128,2048]{1,0:T(8,128)(2,1)} %copy-done.5) | copy-start | bytes 1572868
  289.2 6.6 %copy-start.8 = (bf16[128,2048]{1,0:T(8,128)(2,1)}, bf16[128,2048]{1,0:T(8,128)(2,1)S(1)}, u32[]{:S(2)}) copy-start(bf16[128,2048]{1,0:T(8,128)(2,1)S(1)} %get-tuple-element.22) | copy-start | bytes 1572868
  292.8 0.8 copy-start.2
  303.5 17.6 %copy-start.4 = (bf16[128,2048]{1,0:T(8,128)(2,1)S(1)}, bf16[128,2048]{1,0:T(8,128)(2,1)}, u32[]{:S(2)}) copy-start(bf16[128,2048]{1,0:T(8,128)(2,1)} %fusion.47) | copy-start | bytes 1572868
  303.5 55.3 %copy-start.3 = (bf16[128,2048]{1,0:T(8,128)(2,1)S(1)}, bf16[128,2048]{1,0:T(8,128)(2,1)}, u32[]{:S(2)}) copy-start(bf16[128,2048]{1,0:T(8,128)(2,1)} %copy-done.2) | copy-start | bytes 1572868
  303.6 235.1 %all-gather.8.cloned.1.call-start = ((), (), s32[]{:S(2)}) async-start(), calls=%async_computation.6 | async-start | bytes 8921088 | tf_op jit(solution)/shard_map/all_gather | solution.py:11
  304.3 93.1 %copy-start.7 = (bf16[128,2048]{1,0:T(8,128)(2,1)S(1)}, bf16[128,2048]{1,0:T(8,128)(2,1)}, u32[]{:S(2)}) copy-start(bf16[128,2048]{1,0:T(8,128)(2,1)} %param.21) | copy-start | bytes 1572868
  306.4 114.8 %copy-start.1 = (bf16[128,2048]{1,0:T(8,128)(2,1)S(1)}, bf16[128,2048]{1,0:T(8,128)(2,1)}, u32[]{:S(2)}) copy-start(bf16[128,2048]{1,0:T(8,128)(2,1)} %param.19) | copy-start | bytes 1572868
  306.4 48.2 %all-to-all-start = ((bf16[128,32,64]{0,2,1:T(8,128)(2,1)}), bf16[128,32,64]{0,2,1:T(8,128)(2,1)S(1)}, u32[]{:S(2)}, u32[]{:S(2)}) async-start(bf16[128,32,64]{0,2,1:T(8,128)(2,1)} %bitcast.3), calls=%async_computation | async-start | bytes 1048576 | tf_op jit(solution)/shard_map/all_to_all | solution.py:142
  354.6 82.4 %copy-start.9 = (bf16[128,2048]{1,0:T(8,128)(2,1)S(1)}, bf16[128,2048]{1,0:T(8,128)(2,1)}, u32[]{:S(2)}) copy-start(bf16[128,2048]{1,0:T(8,128)(2,1)} %copy-done.8) | copy-start | bytes 1572868
  354.6 37.7 %all-to-all-start.2 = ((bf16[128,32,64]{0,2,1:T(8,128)(2,1)}), bf16[128,32,64]{0,2,1:T(8,128)(2,1)S(1)}, u32[]{:S(2)}, u32[]{:S(2)}) async-start(bf16[128,32,64]{0,2,1:T(8,128)(2,1)} %bitcast.7), calls=%async_computation.2 | async-start | bytes 1048576 | tf_op jit(solution)/shard_map/all_to_all | solution.py:137
  392.3 38.6 %all-to-all-start.1 = ((bf16[128,32,64]{0,2,1:T(8,128)(2,1)}), bf16[128,32,64]{0,2,1:T(8,128)(2,1)}, u32[]{:S(2)}, u32[]{:S(2)}) async-start(bf16[128,32,64]{0,2,1:T(8,128)(2,1)} %bitcast.5), calls=%async_computation.1 | async-start | bytes 1048576 | tf_op jit(solution)/shard_map/all_to_all | solution.py:143
  398.4 140.3 %copy-start.13 = (f32[64,176]{1,0:T(8,128)S(1)}, f32[64,176]{1,0:T(8,128)}, u32[]{:S(2)}) copy-start(f32[64,176]{1,0:T(8,128)} %param.30) | copy-start | bytes 135172
  430.9 120.8 %all-to-all-start.3 = ((bf16[128,32,64]{0,2,1:T(8,128)(2,1)}), bf16[128,32,64]{0,2,1:T(8,128)(2,1)S(1)}, u32[]{:S(2)}, u32[]{:S(2)}) async-start(bf16[128,32,64]{0,2,1:T(8,128)(2,1)} %bitcast.9), calls=%async_computation.3 | async-start | bytes 1048576 | tf_op jit(solution)/shard_map/all_to_all | solution.py:138
  437.0 104.2 %copy-start.14 = (f32[64,176]{1,0:T(8,128)S(1)}, f32[64,176]{1,0:T(8,128)}, u32[]{:S(2)}) copy-start(f32[64,176]{1,0:T(8,128)} %param.31) | copy-start | bytes 135172
  439.8 104.0 %copy-start.15 = (f32[64,176]{1,0:T(8,128)S(1)}, f32[64,176]{1,0:T(8,128)}, u32[]{:S(2)}) copy-start(f32[64,176]{1,0:T(8,128)} %param.33) | copy-start | bytes 135172
  439.8 106.6 %copy-start.16 = (f32[64,176]{1,0:T(8,128)S(1)}, f32[64,176]{1,0:T(8,128)}, u32[]{:S(2)}) copy-start(f32[64,176]{1,0:T(8,128)} %param.34) | copy-start | bytes 135172
  541.2 7.8 %copy-start.17 = (f32[176,64]{0,1:T(8,128)S(1)}, f32[176,64]{0,1:T(8,128)}, u32[]{:S(2)}) copy-start(f32[176,64]{0,1:T(8,128)} %param.32) | copy-start | bytes 135172
  546.4 5.3 copy-start.18
Sparse Core Ops, SparseCore 0:
  10.7 76.7 all-gather.5
  90.1 69.8 all-gather.3
  174.2 113.2 all-reduce.6
  303.7 117.5 all-reduce.4
  423.1 115.4 all-gather.7
where the time goes:
time: 562 us; the launch traced here: 561 us
  waiting for transfers between devices  447 us (80%)
  matrix products  41.5 us (7%)
  starting transfers between devices  30.4 us (5%)
  other arithmetic  22 us (4%)
  between operations  14 us (2%)
  local copies, waits for them, and re-layouts  6.1 us (1%)
    all_gather x2, waiting for transfers between devices, sent_together(): whole, at, outs = (lax.all_gather(both, axis, axis=dim, tiled=True), 0, [])  169 us
    psum x2, waiting for transfers between devices, block_forward(): lax.psum(jnp.dot(hidden, w_down, preferred_element_type=jnp.float32).asty...  133 us
    all_gather x1, waiting for transfers between devices, gather_turned(): whole = lax.all_gather(both, axis, axis=0, tiled=True)  71.3 us
    all_to_all x1, waiting for transfers between devices, per_device(): lax.all_to_all(saved_second[0], 'fs', split_axis=1, concat_axis=0, tiled=...  32.5 us
    all_to_all x1, waiting for transfers between devices, per_device(): lax.all_to_all(saved_first[0], 'fs', split_axis=1, concat_axis=0, tiled=T...  32.5 us
    all_to_all x1, starting transfers between devices, per_device(): lax.all_to_all(saved_first[0], 'fs', split_axis=1, concat_axis=0, tiled=T...  14.7 us
  transfers between devices with their start and end apart: 9, of which 8 were waited for; matrix products, arithmetic and copies ran while one was open for 6% of the time, Pallas kernels for 0%

commit v1 on v0

--- a/solution.py
+++ b/solution.py
@@ -42,8 +42,11 @@
     gate_pre = jnp.dot(normed, w_gate, preferred_element_type=jnp.float32)
     up_pre = jnp.dot(normed, w_up, preferred_element_type=jnp.float32)
     hidden = (jax.nn.silu(gate_pre) * up_pre).astype(jnp.bfloat16)
-    branch = lax.psum(
-        jnp.dot(hidden, w_down, preferred_element_type=jnp.float32).astype(jnp.bfloat16), "tp"
+    branch = jnp.sum(
+        lax.all_gather(
+            jnp.dot(hidden, w_down, preferred_element_type=jnp.float32).astype(jnp.bfloat16), "tp"
+        ),
+        axis=0,
     ).astype(jnp.float32)
     return (widened + 0.5 * branch).astype(jnp.bfloat16)
 

time: 562 us -> 709 us (1.26)
  waiting for transfers between devices: 447 us -> 585 us
  other arithmetic: 22 us -> 33.1 us
    all_gather x0 -> x2, waiting for transfers between devices: none -> 150 us  [block_forward(): lax.all_gather(jnp.dot(hidden, w_down, preferred_element_type=jnp.float32...]
    psum x2, waiting for transfers between devices: 133 us -> 114 us  [block_backward(): lax.psum(partial_value.astype(jnp.bfloat16), 'tp').astype(jnp.float32)]
    reduce_sum x0 -> x2, other arithmetic: none -> 11.4 us  [block_forward(): jnp.sum(lax.all_gather(jnp.dot(hidden, w_down, preferred_element_type=jnp...]
    all_to_all x1, waiting for transfers between devices: 8.3 us -> 18.9 us  [per_device(): lax.all_to_all(saved_first[1], 'fs', split_axis=1, concat_axis=0, tiled=T...]
  transfers between devices with their start and end apart: 9 -> 11, of which waited for: 8 -> 10; matrix products, arithmetic and copies ran while one was open for 6% -> 9% of each run, Pallas kernels for 0% -> 0%
where the time goes in v1:
time: 709 us; the launch traced here: 708 us
  waiting for transfers between devices  585 us (83%)
  matrix products  40.1 us (6%)
  other arithmetic  33.1 us (5%)
  starting transfers between devices  26.6 us (4%)
  between operations  14.4 us (2%)
  local copies, waits for them, and re-layouts  8.61 us (1%)
    all_gather x2, waiting for transfers between devices, sent_together(): whole, at, outs = (lax.all_gather(both, axis, axis=dim, tiled=True), 0, [])  166 us
    all_gather x2, waiting for transfers between devices, block_forward(): lax.all_gather(jnp.dot(hidden, w_down, preferred_element_type=jnp.float32...  150 us
    psum x2, waiting for transfers between devices, block_backward(): lax.psum(partial_value.astype(jnp.bfloat16), 'tp').astype(jnp.float32)  114 us
    all_gather x1, waiting for transfers between devices, gather_turned(): whole = lax.all_gather(both, axis, axis=0, tiled=True)  72.5 us
    all_to_all x1, waiting for transfers between devices, per_device(): lax.all_to_all(saved_second[0], 'fs', split_axis=1, concat_axis=0, tiled=...  32.5 us
    all_to_all x1, waiting for transfers between devices, per_device(): lax.all_to_all(saved_first[0], 'fs', split_axis=1, concat_axis=0, tiled=T...  31.5 us
    all_to_all x1, waiting for transfers between devices, per_device(): lax.all_to_all(saved_first[1], 'fs', split_axis=1, concat_axis=0, tiled=T...  18.9 us
  transfers between devices with their start and end apart: 11, of which 10 were waited for; matrix products, arithmetic and copies ran while one was open for 9% of the time, Pallas kernels for 0%

profile of v1, /device:TPU:1, one launch (start us, length us, event | category | flops | bytes accessed | tf_op | source)
XLA Modules:
  0.0 707.5 jit_solution(12404322404854150379)
XLA Ops:
  7.2 1.5 pad_maximum_fusion.1
  8.8 1.6 pad_maximum_fusion
  10.4 1.2 fusion.61
  11.6 1.2 fusion.53
  12.9 2.0 fusion.47
  14.9 72.5 %all-gather.10.cloned.1.call-done = bf16[2048,352]{1,0:T(8,128)(2,1)} async-done(((bf16[64,352]{1,0:T(8,128)(2,1)}), bf16[2048,352]{1,0:T(8,128)(2,1)}) %all-gather.10.cloned.1.call-update) | async-done | bytes 1441808 | tf_op jit(solution)/shard_map/all_gather | solution.py:22
  87.5 2.1 fusion.20
  89.6 70.4 %all-gather.8.cloned.1.call-done = bf16[2048,704]{1,0:T(8,128)(2,1)} async-done(((bf16[64,704]{1,0:T(8,128)(2,1)}), bf16[2048,704]{1,0:T(8,128)(2,1)}) %all-gather.8.cloned.1.call-update) | async-done | bytes 2883600 | tf_op jit(solution)/shard_map/all_gather | solution.py:11
  160.0 2.6 fusion.74
  162.6 2.6 constant_dynamic-update-slice_fusion.3
  166.7 1.5 fusion
  168.2 1.6 fusion.93
  169.8 3.9 convolution_convert_fusion.1
  173.8 1.2 fusion.60
  175.0 1.2 fusion.54
  177.1 1.0 fusion.85
  178.1 101.3 %all-reduce.3.cloned.1.call-done = bf16[128,2048]{1,0:T(8,128)(2,1)} async-done(((bf16[128,2048]{1,0:T(8,128)(2,1)}), bf16[128,2048]{1,0:T(8,128)(2,1)}) %all-reduce.3.cloned.1.call-update) | async-done | bytes 524304 | tf_op jit(solution)/shard_map/psum | solution.py:73
  279.4 1.7 fusion.48
  281.1 1.8 fusion.52
  284.2 1.1 constant_dynamic-update-slice_fusion.1
  286.5 1.5 fusion.1
  288.9 81.5 %all-gather.14.cloned.1.call-done = bf16[2048,2048]{1,0:T(8,128)(2,1)} async-done(((bf16[128,2048]{1,0:T(8,128)(2,1)}), bf16[2048,2048]{1,0:T(8,128)(2,1)}) %all-gather.14.cloned.1.call-update) | async-done | bytes 8388624 | tf_op jit(solution)/shard_map/all_gather | solution.py:46
  370.4 6.1 reduce_sum.79
  376.5 1.5 fusion.65
  378.8 1.1 fusion.82
  379.9 4.0 convolution_convert_fusion
  383.9 2.1 copy.27
  386.0 13.3 %all-to-all-start = ((bf16[128,32,64]{0,2,1:T(8,128)(2,1)}), bf16[128,32,64]{0,2,1:T(8,128)(2,1)S(1)}, u32[]{:S(2)}, u32[]{:S(2)}) async-start(bf16[128,32,64]{0,2,1:T(8,128)(2,1)} %bitcast.5), calls=%async_computation | async-start | bytes 1048576 | tf_op jit(solution)/shard_map/all_to_all | solution.py:145
  399.4 2.1 copy.31
  401.4 31.5 %all-to-all-done = bf16[128,32,64]{0,2,1:T(8,128)(2,1)S(1)} async-done(((bf16[128,32,64]{0,2,1:T(8,128)(2,1)}), bf16[128,32,64]{0,2,1:T(8,128)(2,1)S(1)}, u32[]{:S(2)}, u32[]{:S(2)}) %all-to-all-start) | async-done | bytes 524320 | tf_op jit(solution)/shard_map/all_to_all | solution.py:145
  432.9 4.0 all-to-all-start.2
  436.9 1.0 copy.29
  437.9 32.5 %all-to-all-done.2 = bf16[128,32,64]{0,2,1:T(8,128)(2,1)S(1)} async-done(((bf16[128,32,64]{0,2,1:T(8,128)(2,1)}), bf16[128,32,64]{0,2,1:T(8,128)(2,1)S(1)}, u32[]{:S(2)}, u32[]{:S(2)}) %all-to-all-start.2) | async-done | bytes 524320 | tf_op jit(solution)/shard_map/all_to_all | solution.py:140
  470.5 4.5 all-to-all-start.1
  475.9 12.3 %all-reduce.5.cloned.1.call-done = bf16[128,2048]{1,0:T(8,128)(2,1)} async-done(((bf16[128,2048]{1,0:T(8,128)(2,1)}), bf16[128,2048]{1,0:T(8,128)(2,1)}) %all-reduce.5.cloned.1.call-update) | async-done | bytes 524304 | tf_op jit(solution)/shard_map/psum | solution.py:73
  488.2 1.4 fusion.55
  489.6 18.9 %all-to-all-done.1 = bf16[128,32,64]{0,2,1:T(8,128)(2,1)S(1)} async-done(((bf16[128,32,64]{0,2,1:T(8,128)(2,1)}), bf16[128,32,64]{0,2,1:T(8,128)(2,1)S(1)}, u32[]{:S(2)}, u32[]{:S(2)}) %all-to-all-start.1) | async-done | bytes 524320 | tf_op jit(solution)/shard_map/all_to_all | solution.py:146
  508.5 4.3 all-to-all-start.3
  512.8 2.3 fusion.59
  515.1 95.5 %all-gather.12.cloned.1.call-done = bf16[4096,1056]{0,1:T(8,128)(2,1)} async-done(((bf16[128,1056]{0,1:T(8,128)(2,1)}), bf16[4096,1056]{0,1:T(8,128)(2,1)}) %all-gather.12.cloned.1.call-update) | async-done | bytes 8650768 | tf_op jit(solution)/shard_map/all_gather | solution.py:11
  610.7 2.6 fusion.23
  613.2 2.6 fusion.26
  615.9 2.6 fusion.35
  618.4 2.6 fusion.38
  621.1 2.6 fusion.32
  623.6 2.6 fusion.44
  626.2 68.2 %all-gather.16.cloned.1.call-done = bf16[2048,2048]{1,0:T(8,128)(2,1)} async-done(((bf16[128,2048]{1,0:T(8,128)(2,1)}), bf16[2048,2048]{1,0:T(8,128)(2,1)}) %all-gather.16.cloned.1.call-update) | async-done | bytes 8388624 | tf_op jit(solution)/shard_map/all_gather | solution.py:46
  694.4 5.3 reduce_sum.81
  (68 shorter events, 8.7 us)
Async XLA Ops:
  7.2 80.3 %all-gather.10.cloned.1.call-start = ((), (), s32[]{:S(2)}) async-start(), calls=%async_computation.5 | async-start | bytes 1622016 | tf_op jit(solution)/shard_map/all_gather | solution.py:22
  8.7 151.3 %all-gather.8.cloned.1.call-start = ((), (), s32[]{:S(2)}) async-start(), calls=%async_computation.4 | async-start | bytes 3244032 | tf_op jit(solution)/shard_map/all_gather | solution.py:11
  10.4 269.1 %all-reduce.3.cloned.1.call-start = ((), (), s32[]{:S(2)}) async-start(), calls=%async_computation.6 | async-start | bytes 1048576 | tf_op jit(solution)/shard_map/psum | solution.py:73
  160.0 6.0 copy-start
  165.2 3.0 copy-start.12
  165.3 0.7 copy-start.10
  168.2 202.2 %all-gather.14.cloned.1.call-start = ((), (), s32[]{:S(2)}) async-start(), calls=%async_computation.9 | async-start | bytes 8912896 | tf_op jit(solution)/shard_map/all_gather | solution.py:46
  169.8 109.6 %copy-start.11 = (f32[2048]{0:T(1024)S(1)}, f32[2048]{0:T(1024)}, u32[]{:S(2)}) copy-start(f32[2048]{0:T(1024)} %param.23) | copy-start | bytes 24580
  173.7 314.4 %all-reduce.5.cloned.1.call-start = ((), (), s32[]{:S(2)}) async-start(), calls=%async_computation.7 | async-start | bytes 1048576 | tf_op jit(solution)/shard_map/psum | solution.py:73
  176.3 0.8 copy-start.4
  279.4 4.2 copy-start.9
  279.4 4.8 copy-start.5
  282.9 0.8 copy-start.2
  288.0 322.7 %all-gather.12.cloned.1.call-start = ((), (), s32[]{:S(2)}) async-start(), calls=%async_computation.8 | async-start | bytes 8921088 | tf_op jit(solution)/shard_map/all_gather | solution.py:11
  288.7 405.8 %all-gather.16.cloned.1.call-start = ((), (), s32[]{:S(2)}) async-start(), calls=%async_computation.10 | async-start | bytes 8912896 | tf_op jit(solution)/shard_map/all_gather | solution.py:46
  378.0 0.8 copy-start.6
  383.9 53.1 %copy-start.3 = (bf16[128,2048]{1,0:T(8,128)(2,1)S(1)}, bf16[128,2048]{1,0:T(8,128)(2,1)}, u32[]{:S(2)}) copy-start(bf16[128,2048]{1,0:T(8,128)(2,1)} %copy-done.2) | copy-start | bytes 1572868
  383.9 91.0 %copy-start.8 = (bf16[128,2048]{1,0:T(8,128)(2,1)S(1)}, bf16[128,2048]{1,0:T(8,128)(2,1)}, u32[]{:S(2)}) copy-start(bf16[128,2048]{1,0:T(8,128)(2,1)} %param.21) | copy-start | bytes 1572868
  386.0 102.2 %copy-start.1 = (bf16[128,2048]{1,0:T(8,128)(2,1)S(1)}, bf16[128,2048]{1,0:T(8,128)(2,1)}, u32[]{:S(2)}) copy-start(bf16[128,2048]{1,0:T(8,128)(2,1)} %param.19) | copy-start | bytes 1572868
  386.0 46.8 %all-to-all-start = ((bf16[128,32,64]{0,2,1:T(8,128)(2,1)}), bf16[128,32,64]{0,2,1:T(8,128)(2,1)S(1)}, u32[]{:S(2)}, u32[]{:S(2)}) async-start(bf16[128,32,64]{0,2,1:T(8,128)(2,1)} %bitcast.5), calls=%async_computation | async-start | bytes 1048576 | tf_op jit(solution)/shard_map/all_to_all | solution.py:145
  432.9 37.6 %all-to-all-start.2 = ((bf16[128,32,64]{0,2,1:T(8,128)(2,1)}), bf16[128,32,64]{0,2,1:T(8,128)(2,1)S(1)}, u32[]{:S(2)}, u32[]{:S(2)}) async-start(bf16[128,32,64]{0,2,1:T(8,128)(2,1)} %bitcast.9), calls=%async_computation.2 | async-start | bytes 1048576 | tf_op jit(solution)/shard_map/all_to_all | solution.py:140
  470.5 140.2 %copy-start.13 = (f32[64,176]{1,0:T(8,128)S(1)}, f32[64,176]{1,0:T(8,128)}, u32[]{:S(2)}) copy-start(f32[64,176]{1,0:T(8,128)} %param.30) | copy-start | bytes 135172
  470.5 38.0 %all-to-all-start.1 = ((bf16[128,32,64]{0,2,1:T(8,128)(2,1)}), bf16[128,32,64]{0,2,1:T(8,128)(2,1)S(1)}, u32[]{:S(2)}, u32[]{:S(2)}) async-start(bf16[128,32,64]{0,2,1:T(8,128)(2,1)} %bitcast.7), calls=%async_computation.1 | async-start | bytes 1048576 | tf_op jit(solution)/shard_map/all_to_all | solution.py:146
  475.9 137.3 %copy-start.14 = (f32[64,176]{1,0:T(8,128)S(1)}, f32[64,176]{1,0:T(8,128)}, u32[]{:S(2)}) copy-start(f32[64,176]{1,0:T(8,128)} %param.31) | copy-start | bytes 135172
  508.5 115.2 %all-to-all-start.3 = ((bf16[128,32,64]{0,2,1:T(8,128)(2,1)}), bf16[128,32,64]{0,2,1:T(8,128)(2,1)S(1)}, u32[]{:S(2)}, u32[]{:S(2)}) async-start(bf16[128,32,64]{0,2,1:T(8,128)(2,1)} %bitcast.11), calls=%async_computation.3 | async-start | bytes 1048576 | tf_op jit(solution)/shard_map/all_to_all | solution.py:141
  512.8 103.0 %copy-start.15 = (f32[64,176]{1,0:T(8,128)S(1)}, f32[64,176]{1,0:T(8,128)}, u32[]{:S(2)}) copy-start(f32[64,176]{1,0:T(8,128)} %param.33) | copy-start | bytes 135172
  515.1 103.3 %copy-start.16 = (f32[64,176]{1,0:T(8,128)S(1)}, f32[64,176]{1,0:T(8,128)}, u32[]{:S(2)}) copy-start(f32[64,176]{1,0:T(8,128)} %param.34) | copy-start | bytes 135172
  613.2 7.8 %copy-start.17 = (f32[176,64]{0,1:T(8,128)S(1)}, f32[176,64]{0,1:T(8,128)}, u32[]{:S(2)}) copy-start(f32[176,64]{0,1:T(8,128)} %param.32) | copy-start | bytes 135172
  618.4 5.2 copy-start.18
  694.4 5.3 copy-start.7
Sparse Core Ops, SparseCore 0:
  10.7 76.7 all-gather.9
  90.1 69.8 all-gather.7
  168.3 111.0 all-reduce.2
  282.9 87.4 all-gather.13
  373.4 114.7 all-reduce.4
  490.1 120.5 all-gather.11
  614.2 80.1 all-gather.15
